TPU v7x, 512 devices: a whole 4x4x16 slice. The times are simulated.
512 devices in a mesh: sp: 128 (over z, x, core), tp: 4 (over y).
Axes of the slice: x: 4, y: 4, z: 16, core: 2. Of those that a mesh axis runs over, the one named last changes fastest.
Arguments:
- inputs: bfloat16 [4, 16384, 1024], P(None, 'sp'), may hold values from -6 to 6
- norm_gain: float32 [1024], replicated, may hold values from 0.1 to 1.9
- query_weight: bfloat16 [1024, 3, 8, 64], P('sp', None, 'tp'), may hold values from -0.1875 to 0.1875
- key_weight: bfloat16 [1024, 3, 8, 64], P('sp', None, 'tp'), may hold values from -0.1875 to 0.1875
- value_weight: bfloat16 [1024, 3, 8, 64], P('sp', None, 'tp'), may hold values from -0.1875 to 0.1875
- query_gain: float32 [3, 64], replicated, may hold values from 0.1 to 1.9
- key_gain: float32 [3, 64], replicated, may hold values from 0.1 to 1.9
- out_weight: bfloat16 [8, 64, 1024], P('tp', None, 'sp'), may hold values from -0.75 to 0.75
Outputs:
- mixed: bfloat16 [4, 16384, 1024], P(None, 'sp', 'tp')
All inputs are finite; a program needn't handle non-finite values.
Results may differ from a plain program's by a relative error of at most 0.02.
Values may be sent and summed in bfloat16 or wider, within the bound.
A program may use at most 64 MiB of HBM per device.

v0:
```python
import math

import jax
import jax.numpy as jnp
from jax import lax
from jax.sharding import Mesh
from jax.sharding import PartitionSpec as P

SPAN_CLOSE = 32
SPREAD_CENTRAL = 4
SPAN_CENTRAL = 32
SPREAD_DISTANT = 16
SPAN_DISTANT = 16
SP = ("sp_0", "sp_1", "sp_2")


eps = 1e-06
neg_fill = -1e30


def joined_along(tiles, dim):
    tiles = jnp.moveaxis(tiles, 0, dim)
    shape = tiles.shape
    return tiles.reshape(*shape[:dim], shape[dim] * shape[dim + 1], *shape[dim + 2 :])


def stacked_from(value, axes, sequence):
    tiles = value[None]
    for k in sequence:
        tiles = lax.all_gather(tiles, axes[k], axis=0, tiled=True)
    block = [lax.axis_size(axes[k]) for k in reversed(sequence)]
    tiles = tiles.reshape(*block, *value.shape)
    turned = sorted(range(len(sequence)), key=lambda place: sequence[len(sequence) - 1 - place])
    return tiles.transpose(*turned, *range(len(sequence), tiles.ndim)).reshape(-1, *value.shape)


def gather_axes(value, axes, sequence, dim):
    return joined_along(stacked_from(value, axes, sequence), dim)


def over_axes(value, axes, sequence, dim, take_in, carry):
    everything = jax.tree.map(lambda part: gather_axes(part, axes, sequence, dim), value)
    return take_in(carry, everything, jnp.int32(0))


def padded(cells, sides, width, closed):
    for axis, dim in sides:
        count = lax.axis_size(axis)
        ends = count if closed else count - 1
        head = lax.slice_in_dim(cells, 0, width, axis=dim)
        tail = lax.slice_in_dim(cells, cells.shape[dim] - width, cells.shape[dim], axis=dim)
        cells = jnp.concatenate(
            [
                lax.ppermute(tail, axis, [(i, (i + 1) % count) for i in range(ends)]),
                cells,
                lax.ppermute(head, axis, [((i + 1) % count, i) for i in range(ends)]),
            ],
            axis=dim,
        )
    return cells


def shifted(block, axis, distance):
    devices = range(lax.axis_size(axis))
    route = [(i - distance, i) for i in devices if i - distance in devices]
    return lax.ppermute(block, axis, route)


def on_whole(value, axes, sequence, dim, apply):
    return apply(gather_axes(value, axes, sequence, dim), jnp.int32(0))


def row_norm(values, gain):
    scaled = values * lax.rsqrt(jnp.mean(values * values, axis=-1, keepdims=True) + eps)
    return scaled * gain


def band_attend(queries, keys, values, margin, dilation, half, slopes, anchor, seq_len):
    batch, count, heads, width = queries.shape
    query_rows = count // dilation
    key_rows = query_rows + 2 * half
    first = margin - half * dilation
    keys = keys[:, first : first + key_rows * dilation]
    values = values[:, first : first + key_rows * dilation]
    query_sub = queries.reshape(batch, query_rows, dilation, heads, width)
    key_sub = keys.reshape(batch, key_rows, dilation, heads, width)
    value_sub = values.reshape(batch, key_rows, dilation, heads, width)
    scores = jnp.einsum(
        "barhe,bcrhe->brhac", query_sub, key_sub, precision=lax.Precision.DEFAULT
    ) / math.sqrt(width)
    offset = jnp.arange(key_rows)[None, :] - half - jnp.arange(query_rows)[:, None]
    key_place = (
        anchor + first + dilation * jnp.arange(key_rows)[None, :] + jnp.arange(dilation)[:, None]
    )
    inside = (key_place >= 0) & (key_place < seq_len)
    allowed = (jnp.abs(offset) <= half)[None, :, :] & inside[:, None, :]
    slant = -slopes[:, None, None] * (jnp.abs(offset).astype(jnp.float32) / float(half))[None]
    scores = jnp.where(allowed[None, :, None], scores + slant[None, None], neg_fill)
    log_total = jax.nn.logsumexp(scores, axis=-1)
    weights = jnp.exp(scores - log_total[..., None])
    result = jnp.einsum("brhac,bcrhe->barhe", weights, value_sub, precision=lax.Precision.DEFAULT)
    log_total = jnp.transpose(log_total, (0, 3, 1, 2)).reshape(batch, count, heads)
    return (result.reshape(batch, count, heads, width), log_total)


def assemble(own, fetched, reach):
    before = [fetched[distance] for distance in range(reach, 0, -1)]
    after = [fetched[-distance] for distance in range(1, reach + 1)]
    return jnp.concatenate(before + [own] + after, axis=1)


def body(
    inputs, norm_gain, query_weight, key_weight, value_weight, query_gain, key_gain, out_weight
):
    batch, local_sequence_count, model_width = inputs.shape
    groups = query_weight.shape[1]
    heads_here = query_weight.shape[2]
    head_width = query_weight.shape[3]
    seq_len = local_sequence_count * lax.axis_size(SP)
    place = lax.axis_index(SP) * local_sequence_count
    flat = inputs.reshape(batch * local_sequence_count, model_width).astype(jnp.float32)
    normed = row_norm(flat, norm_gain).astype(jnp.bfloat16)
    empty = jnp.zeros((batch * local_sequence_count, groups * heads_here * head_width), jnp.float32)

    def add_rows(totals, pieces, start):
        rows = pieces[0].shape[0]
        columns = lax.dynamic_slice_in_dim(normed, start, rows, 1)
        return tuple(
            (
                total
                + jnp.dot(columns, piece.reshape(rows, -1), preferred_element_type=jnp.float32)
                for total, piece in zip(totals, pieces)
            )
        )

    projected = over_axes(
        (query_weight, key_weight, value_weight),
        (("sp_0", "sp_1"), "sp_2"),
        (0, 1),
        0,
        add_rows,
        (empty, empty, empty),
    )
    layout = (batch, local_sequence_count, groups, heads_here, head_width)
    queries = projected[0].astype(jnp.bfloat16).reshape(layout)
    keys = projected[1].astype(jnp.bfloat16).reshape(layout)
    values = projected[2].astype(jnp.bfloat16).reshape(layout)
    pairs = jnp.concatenate([keys, values], axis=-1)
    total_heads = heads_here * lax.axis_size("tp")
    head_index = lax.axis_index("tp") * heads_here + jnp.arange(heads_here)
    slopes = jnp.exp2(-8.0 * (head_index + 1).astype(jnp.float32) / total_heads)
    central_extent = (
        SPREAD_CENTRAL * SPAN_CENTRAL + local_sequence_count - 1
    ) // local_sequence_count
    distant_extent = (
        SPREAD_DISTANT * SPAN_DISTANT + local_sequence_count - 1
    ) // local_sequence_count
    near_window = padded(pairs[:, :, 0], ((SP, 1),), SPAN_CLOSE, False)
    mid_fetched = {}
    far_fetched = {}
    for distance in range(1, central_extent + 1):
        for direction in (1, -1):
            both = shifted(pairs[:, :, 1:], SP, direction * distance)
            mid_fetched[direction * distance] = both[:, :, 0]
            far_fetched[direction * distance] = both[:, :, 1]
    for distance in range(central_extent + 1, distant_extent + 1):
        for direction in (1, -1):
            far_fetched[direction * distance] = shifted(pairs[:, :, 2], SP, direction * distance)
    central_span_width = assemble(pairs[:, :, 1], mid_fetched, central_extent)
    distant_span_width = assemble(pairs[:, :, 2], far_fetched, distant_extent)
    settings = (
        (near_window, SPAN_CLOSE, 1, SPAN_CLOSE),
        (central_span_width, central_extent * local_sequence_count, SPREAD_CENTRAL, SPAN_CENTRAL),
        (distant_span_width, distant_extent * local_sequence_count, SPREAD_DISTANT, SPAN_DISTANT),
    )
    results = []
    totals = []
    for group in range(3):
        window, margin, dilation, half = settings[group]
        query_group = row_norm(queries[:, :, group].astype(jnp.float32), query_gain[group])
        key_group = row_norm(window[..., :head_width].astype(jnp.float32), key_gain[group])
        value_group = window[..., head_width:].astype(jnp.float32)
        result, log_total = band_attend(
            query_group,
            key_group,
            value_group,
            margin,
            dilation,
            half,
            slopes,
            place - margin,
            seq_len,
        )
        results.append(result)
        totals.append(log_total)
    weights = jax.nn.softmax(jnp.stack(totals, 0), axis=0)
    combined = jnp.sum(weights[..., None] * jnp.stack(results, 0), axis=0)
    merged = combined.astype(jnp.bfloat16).reshape(
        batch * local_sequence_count, heads_here * head_width
    )

    def project(piece, start):
        return jnp.dot(merged, piece, preferred_element_type=jnp.float32)

    terms = on_whole(out_weight.reshape(heads_here * head_width, -1), SP, (0, 1, 2), 1, project)
    summed = lax.psum_scatter(
        terms.astype(jnp.bfloat16), "tp", scatter_dimension=1, tiled=True
    ).astype(jnp.float32)
    return summed.astype(jnp.bfloat16).reshape(batch, local_sequence_count, -1)


def solution(mesh):
    finer = Mesh(mesh.devices.reshape(16, 4, 2, mesh.shape["tp"]), ("sp_0", "sp_1", "sp_2", "tp"))
    placed = (
        P(None, SP, None),
        P(),
        P(SP, None, "tp", None),
        P(SP, None, "tp", None),
        P(SP, None, "tp", None),
        P(),
        P(),
        P("tp", None, SP),
    )
    return jax.shard_map(
        body, mesh=finer, in_specs=placed, out_specs=P(None, SP, "tp"), check_vma=False
    )
```

profile of v0, /device:TPU:1, one launch (start us, length us, event | category | flops | bytes accessed | tf_op | source)
XLA Modules:
  0.0 473.2 jit_solution(8545988568318055102)
XLA Ops:
  6.5 1.5 fusion.2
  8.0 82.1 %all-gather.1 = bf16[512,3,2,64]{3,2,1,0:T(2,128)(2,1)S(1)} all-gather(bf16[8,3,2,64]{3,2,1,0:T(2,128)(2,1)} %param.11), channel_id=3, replica_groups=mesh['sp_0'=16,'sp_1'=4,'sp_2'=2,'tp'=4] {'sp_0','sp_1'}, dimensions={0}, use_global_device_ids=true | all-gather | bytes 399360 | tf_op jit(solution)/shard_map/all_gather | solution.py:30
  90.3 29.2 %all_gather.30 = bf16[128,8,3,2,64]{4,1,3,2,0:T(8,128)(2,1)S(1)} all-gather(bf16[64,8,3,2,64]{4,1,3,2,0:T(8,128)(2,1)S(1)} %copy.215), channel_id=1, replica_groups=mesh['sp_0'=16,'sp_1'=4,'sp_2'=2,'tp'=4] {'sp_2'}, dimensions={0}, use_global_device_ids=true | all-gather | bytes 1179648 | tf_op jit(solution)/shard_map/all_gather | solution.py:30
  119.5 1.2 copy.329
  120.8 1.0 reshape_reshape_reshape.10
  121.8 73.6 %all-gather.2 = bf16[512,3,2,64]{3,2,1,0:T(2,128)(2,1)S(1)} all-gather(bf16[8,3,2,64]{3,2,1,0:T(2,128)(2,1)S(1)} %copy-done.10), channel_id=4, replica_groups=mesh['sp_0'=16,'sp_1'=4,'sp_2'=2,'tp'=4] {'sp_0','sp_1'}, dimensions={0}, use_global_device_ids=true | all-gather | bytes 399360 | tf_op jit(solution)/shard_map/all_gather | solution.py:30
  195.5 28.6 %all_gather.32 = bf16[128,8,3,2,64]{4,1,3,2,0:T(8,128)(2,1)S(1)} all-gather(bf16[64,8,3,2,64]{4,1,3,2,0:T(8,128)(2,1)S(1)} %copy.219), channel_id=1, replica_groups=mesh['sp_0'=16,'sp_1'=4,'sp_2'=2,'tp'=4] {'sp_2'}, dimensions={0}, use_global_device_ids=true | all-gather | bytes 1179648 | tf_op jit(solution)/shard_map/all_gather | solution.py:30
  224.1 1.2 copy.328
  225.4 1.7 reshape_reshape_reshape.11
  227.5 0.8 copy-done.5
  230.2 1.0 copy.223
  231.6 1.0 copy.224
  232.6 0.8 fusion.57
  233.4 1.4 collective-permute-start.5
  234.8 4.7 collective-permute-start.4
  239.5 0.8 fusion.92
  240.3 2.1 collective-permute-start
  242.3 3.1 collective-permute-start.1
  245.4 0.8 fusion.43
  246.2 1.9 collective-permute-start.3
  252.8 22.9 %all_gather.33 = bf16[16,128,8]{1,2,0:T(8,128)(2,1)S(1)} all-gather(bf16[1,128,8]{1,2,0:T(8,128)(2,1)S(1)} %broadcast_in_dim_reshape.3), channel_id=1, replica_groups=mesh['sp_0'=16,'sp_1'=4,'sp_2'=2,'tp'=4] {'sp_0'}, dimensions={0}, use_global_device_ids=true | all-gather | bytes 34816 | tf_op jit(solution)/shard_map/all_gather | solution.py:30
  275.7 0.8 broadcast_multiply_fusion
  276.5 9.2 %all_gather.34 = bf16[64,128,8]{1,2,0:T(8,128)(2,1)S(1)} all-gather(bf16[16,128,8]{1,2,0:T(8,128)(2,1)S(1)} %all_gather.33), channel_id=1, replica_groups=mesh['sp_0'=16,'sp_1'=4,'sp_2'=2,'tp'=4] {'sp_1'}, dimensions={0}, use_global_device_ids=true | all-gather | bytes 163840 | tf_op jit(solution)/shard_map/all_gather | solution.py:30
  285.7 74.6 %all-gather = bf16[512,3,2,64]{3,2,1,0:T(2,128)(2,1)S(1)} all-gather(bf16[8,3,2,64]{3,2,1,0:T(2,128)(2,1)S(1)} %copy-done.11), channel_id=2, replica_groups=mesh['sp_0'=16,'sp_1'=4,'sp_2'=2,'tp'=4] {'sp_0','sp_1'}, dimensions={0}, use_global_device_ids=true | all-gather | bytes 399360 | tf_op jit(solution)/shard_map/all_gather | solution.py:30
  360.4 38.5 %all_gather.28 = bf16[128,8,3,2,64]{4,1,3,2,0:T(8,128)(2,1)S(1)} all-gather(bf16[64,8,3,2,64]{4,1,3,2,0:T(8,128)(2,1)S(1)} %copy.211), channel_id=1, replica_groups=mesh['sp_0'=16,'sp_1'=4,'sp_2'=2,'tp'=4] {'sp_2'}, dimensions={0}, use_global_device_ids=true | all-gather | bytes 1179648 | tf_op jit(solution)/shard_map/all_gather | solution.py:30
  398.9 1.2 copy.330
  400.1 1.7 reshape_reshape_reshape.9
  401.9 1.8 convolution_convert_fusion.3
  406.4 0.9 multiply_multiply_fusion
  407.3 1.0 multiply_multiply_fusion.1
  408.4 2.1 all_gather.35
  410.5 0.8 copy.260
  411.3 1.9 collective-permute-start.2
  413.2 1.3 pad_maximum_fusion.1
  415.3 1.0 convolution_bitcast_fusion.1
  416.3 1.0 constant_dynamic-update-slice_fusion.2
  417.3 1.0 slice_bitcast_fusion.2
  418.3 1.2 collective-permute-done.2
  420.3 1.6 fusion.94
  423.1 1.0 constant_dynamic-update-slice_fusion.1
  425.1 1.0 fusion.59
  426.1 1.0 constant_dynamic-update-slice_fusion
  427.3 0.9 fusion.8
  428.2 0.8 copy.239
  429.0 1.9 fusion.93
  433.3 0.8 copy.252
  435.7 1.5 convolution_convert_fusion
  437.2 29.1 %reduce-scatter.2.cloned.1.call-done = bf16[512,256]{1,0:T(8,128)(2,1)} async-done(((bf16[512,1024]{1,0:T(8,128)(2,1)}), bf16[512,256]{1,0:T(8,128)(2,1)}) %reduce-scatter.2.cloned.1.call-update) | async-done | bytes 262160 | tf_op jit(solution)/shard_map/reduce_scatter | solution.py:206
  (139 shorter events, 17.9 us)
Async XLA Ops:
  6.5 459.8 %reduce-scatter.2.cloned.1.call-start = ((), (), s32[]{:S(2)}) async-start(), calls=%async_computation.1 | async-start | bytes 1310720 | tf_op jit(solution)/shard_map/reduce_scatter | solution.py:206
  120.8 1.0 copy-start.10
  225.4 1.8 copy-start
  225.4 1.8 copy-start.12
  227.2 1.1 copy-start.5
  227.5 1.5 copy-start.2
  233.4 16.1 %copy-start.16 = (f32[3,64]{1,0:T(4,128)S(1)}, f32[3,64]{1,0:T(4,128)}, u32[]{:S(2)}) copy-start(f32[3,64]{1,0:T(4,128)} %param.13) | copy-start | bytes 2308
  233.4 16.6 %copy-start.17 = (f32[3,64]{1,0:T(4,128)S(1)}, f32[3,64]{1,0:T(4,128)}, u32[]{:S(2)}) copy-start(f32[3,64]{1,0:T(4,128)} %param.14) | copy-start | bytes 2308
  233.4 17.2 %copy-start.13 = (bf16[2,64,8]{1,2,0:T(8,128)(2,1)S(1)}, bf16[2,64,8]{1,2,0:T(8,128)(2,1)}, u32[]{:S(2)}) copy-start(bf16[2,64,8]{1,2,0:T(8,128)(2,1)} %param.15) | copy-start | bytes 6148
  233.4 192.7 %collective-permute-start.5 = (bf16[4,128,2,128]{1,3,2,0:T(8,128)(2,1)}, bf16[4,128,2,128]{1,3,2,0:T(8,128)(2,1)}, u32[]{:S(2)}, u32[]{:S(2)}) collective-permute-start(bf16[4,128,2,128]{1,3,2,0:T(8,128)(2,1)} %get-tuple-element.13), channel_id=1, source_target_pairs={{8,0},{12,4},{16,8},{20,12},{24,16},{28,20},{32,24},{36,28},{40,32... | collective-permute-start | bytes 786440 | tf_op jit(solution)/shard_map/ppermute | solution.py:66
  234.8 181.5 %collective-permute-start.4 = (bf16[4,128,2,128]{1,3,2,0:T(8,128)(2,1)}, bf16[4,128,2,128]{1,3,2,0:T(8,128)(2,1)}, u32[]{:S(2)}, u32[]{:S(2)}) collective-permute-start(bf16[4,128,2,128]{1,3,2,0:T(8,128)(2,1)} %get-tuple-element.13), channel_id=1, source_target_pairs={{0,8},{4,12},{8,16},{12,20},{16,24},{20,28},{24,32},{28,36},{32,40... | collective-permute-start | bytes 786440 | tf_op jit(solution)/shard_map/ppermute | solution.py:66
  240.3 45.4 %copy-start.11 = (bf16[8,3,2,64]{3,2,1,0:T(2,128)(2,1)S(1)}, bf16[8,3,2,64]{3,2,1,0:T(2,128)(2,1)}, u32[]{:S(2)}) copy-start(bf16[8,3,2,64]{3,2,1,0:T(2,128)(2,1)} %param.10) | copy-start | bytes 18436
  240.3 171.0 %collective-permute-start = (bf16[4,32,2,128]{1,3,2,0:T(8,128)(2,1)S(1)}, bf16[4,32,2,128]{1,3,2,0:T(8,128)(2,1)}, u32[]{:S(2)}, u32[]{:S(2)}) collective-permute-start(bf16[4,32,2,128]{1,3,2,0:T(8,128)(2,1)S(1)} %get-tuple-element.20), channel_id=1, source_target_pairs={{0,4},{4,8},{8,12},{12,16},{16,20},{20,24},{24,28},{28,32},{32,36}... | collective-permute-start | bytes 196616 | tf_op jit(solution)/shard_map/ppermute | solution.py:54
  242.3 170.9 %collective-permute-start.1 = (bf16[4,32,2,128]{1,3,2,0:T(8,128)(2,1)}, bf16[4,32,2,128]{1,3,2,0:T(8,128)(2,1)}, u32[]{:S(2)}, u32[]{:S(2)}) collective-permute-start(bf16[4,32,2,128]{1,3,2,0:T(8,128)(2,1)} %get-tuple-element.21), channel_id=1, source_target_pairs={{4,0},{8,4},{12,8},{16,12},{20,16},{24,20},{28,24},{32,28},{36,32}... | collective-permute-start | bytes 196616 | tf_op jit(solution)/shard_map/ppermute | solution.py:56
  246.2 171.0 %collective-permute-start.3 = (bf16[4,128,2,2,128]{1,4,3,0,2:T(8,128)(2,1)}, bf16[4,128,2,2,128]{1,4,3,0,2:T(8,128)(2,1)}, u32[]{:S(2)}, u32[]{:S(2)}) collective-permute-start(bf16[4,128,2,2,128]{1,4,3,0,2:T(8,128)(2,1)} %fusion.43), channel_id=1, source_target_pairs={{4,0},{8,4},{12,8},{16,12},{20,16},{24,20},{28,24},{32,28},{36,32}... | collective-permute-start | bytes 1572872 | tf_op jit(solution)/shard_map/ppermute | solution.py:66
  400.1 1.8 copy-start.3
  403.7 0.8 copy-start.14
  404.5 0.7 copy-start.20
  404.6 1.3 copy-start.18
  404.6 1.9 copy-start.15
  408.4 6.3 %copy-start.6 = (f32[2,128,192]{1,2,0:T(8,128)S(1)}, f32[2,128,192]{1,2,0:T(8,128)}, u32[]{:S(2)}) copy-start(f32[2,128,192]{1,2,0:T(8,128)} %broadcast_multiply_fusion) | copy-start | bytes 589828
  408.4 6.3 %copy-start.8 = (pred[128,192]{0,1:T(8,128)(4,1)S(1)}, pred[128,192]{0,1:T(8,128)(4,1)}, u32[]{:S(2)}) copy-start(pred[128,192]{0,1:T(8,128)(4,1)} %fusion.71) | copy-start | bytes 73732
  408.4 6.3 %copy-start.19 = (f32[64]{0:T(128)S(1)}, f32[64]{0:T(128)}, u32[]{:S(2)}) copy-start(f32[64]{0:T(128)} %get-tuple-element.22) | copy-start | bytes 772
  411.3 8.2 %collective-permute-start.2 = (bf16[4,128,2,2,128]{1,4,3,0,2:T(8,128)(2,1)}, bf16[4,128,2,2,128]{1,4,3,0,2:T(8,128)(2,1)S(1)}, u32[]{:S(2)}, u32[]{:S(2)}) collective-permute-start(bf16[4,128,2,2,128]{1,4,3,0,2:T(8,128)(2,1)} %fusion.43), channel_id=1, source_target_pairs={{0,4},{4,8},{8,12},{12,16},{16,20},{20,24},{24,28},{28,32},{32,36}... | collective-permute-start | bytes 1572872 | tf_op jit(solution)/shard_map/ppermute | solution.py:66
  429.0 2.9 copy-start.7
  434.5 0.7 copy-start.9
  434.6 1.0 copy-start.1
  434.6 1.1 copy-start.4
Sparse Core Ops, SparseCore 0:
  437.3 28.9 reduce-scatter.1
where the time goes:
time: 475 us; the launch traced here: 473 us
  blocking collectives  361 us (76%)
  waiting for transfers between devices  30.4 us (6%)
  local copies, waits for them, and re-layouts  26.4 us (6%)
  other arithmetic  15.9 us (3%)
  starting transfers between devices  15.1 us (3%)
  between operations  14.2 us (3%)
  matrix products  10.5 us (2%)
    all_gather x9, blocking collectives, stacked_from(): tiles = lax.all_gather(tiles, axes[k], axis=0, tiled=True)  361 us
    reduce_scatter x1, waiting for transfers between devices, body(): lax.psum_scatter(terms.astype(jnp.bfloat16), 'tp', scatter_dimension=1, t...  29.1 us
    ppermute x4, starting transfers between devices, shifted(): return lax.ppermute(block, axis, route)  9.94 us
  transfers between devices with their start and end apart: 7, of which 2 were waited for; matrix products, arithmetic and copies ran while one was open for 6% of the time, Pallas kernels for 0%

commit v1 on v0

v1 whole, which is shorter than its diff:
```python
import functools
import math

import jax
import jax.numpy as jnp
from jax import lax
from jax.experimental import pallas as pl
from jax.experimental.pallas import tpu as pltpu
from jax.sharding import Mesh
from jax.sharding import PartitionSpec as P

REACH = (32, 128, 256)
SPREAD = (1, 4, 16)
eps = 1e-06
SP = ("z", "x", "c")
bf16 = jnp.bfloat16
f32 = jnp.float32


def kernel(
    Z, X, Y, L, inputs, weights, norm_gain, gains, out,
    xbuf, wbuf, wfull, xn, qbuf, kv0, kv1, kv2, valid, m0, m1, m2, mout, mbuf, wo,
    x_send, x_recv, in_send, in_recv, in_local,
    r_send, r_recv, l_send, l_recv, dr_send, dr_recv, dl_send, dl_recv,
    h_send, h_recv, o_send, o_recv, y_send, y_recv,
):
    kv = (kv0, kv1, kv2)
    mask = (m0, m1, m2)
    z, x, c, y = (lax.axis_index(a) for a in ("z", "x", "c", "y"))
    half_x = X // 2
    H = Z // 2
    D = Z * X * 16
    rows = X * L
    cols = D // Y
    wide = 1152

    def at(dz=0, dx=0, dc=0, dy=0):
        return {
            "z": lax.rem(z + dz + Z, Z),
            "x": lax.rem(x + dx + X, X),
            "c": lax.rem(c + dc, 2),
            "y": lax.rem(y + dy + Y, Y),
        }

    def remote(src, dst, send, recv, target):
        return pltpu.make_async_remote_copy(
            src_ref=src, dst_ref=dst, send_sem=send, recv_sem=recv,
            device_id=target, device_id_type=pl.DeviceIdType.MESH,
        )

    barrier = pltpu.get_barrier_semaphore()
    count = 0
    for dx in range(X):
        for dc in range(2):
            for dy in range(Y):
                if dx or dc or dy:
                    pl.semaphore_signal(
                        barrier, inc=1, device_id=at(0, dx, dc, dy),
                        device_id_type=pl.DeviceIdType.MESH,
                    )
                    count += 1
    cross = 2 * c - 1
    for target in (at(1), at(-1), at(cross, 0, 1)):
        pl.semaphore_signal(barrier, inc=1, device_id=target, device_id_type=pl.DeviceIdType.MESH)
        count += 1
    pl.semaphore_wait(barrier, count)

    def x_copy(j):
        return remote(weights, wbuf.at[c, z, x], x_send.at[j], x_recv.at[j], at(0, j))

    def slot(zz, j):
        return wbuf.at[c, lax.rem(zz + 2 * Z, Z), lax.rem(x + j, X)]

    def r_copy(k, j, first=False):
        s = slot(z - k, j)
        return remote(weights if first else s, s, r_send.at[k, j], r_recv.at[k, j], at(1))

    def l_copy(k, j, first=False):
        s = slot(z + k, j)
        return remote(weights if first else s, s, l_send.at[k, j], l_recv.at[k, j], at(-1))

    def dr_copy(k):
        s = wbuf.at[c, lax.rem(z - k + Z, Z)]
        return remote(s, s, dr_send.at[k], dr_recv.at[k], at(0, 0, 1))

    def dl_copy(k):
        s = wbuf.at[c, lax.rem(z + k, Z)]
        return remote(s, s, dl_send.at[k], dl_recv.at[k], at(0, 0, 1))

    r_copy(0, 0, True).start()
    l_copy(0, 0, True).start()
    for j in range(1, X):
        x_copy(j).start()

    mine = x // half_x
    place = lax.rem(x, half_x) * 2 + c

    def in_copy(j):
        b = lax.rem(x + j, X)
        target = {"z": z, "x": b, "c": mine, "y": y}
        return remote(inputs.at[b], xbuf.at[place], in_send.at[j], in_recv.at[place], target)

    own_copy = pltpu.make_async_copy(inputs.at[x], xbuf.at[place], in_local)

    @pl.when(mine == c)
    def _():
        own_copy.start()

    @pl.when(mine != c)
    def _():
        in_copy(0).start()

    for j in range(1, X):
        in_copy(j).start()

    wbuf[c, z, x] = weights[...]

    lane = lax.broadcasted_iota(jnp.int32, (1, 128), 1)
    low = lane < 64

    def masks(step):
        size = L // H
        start = pl.multiple_of(step * size, size)
        for g in range(3):
            reach, spread = REACH[g], SPREAD[g]
            shape = (size, L + 2 * reach)
            gap = (
                lax.broadcasted_iota(jnp.int32, shape, 1)
                - lax.broadcasted_iota(jnp.int32, shape, 0)
                - reach
                - start
            )
            far = jnp.abs(gap)
            ok = (far <= reach) & ((gap & (spread - 1)) == 0)
            far = far.astype(f32) * (1.0 / reach)
            for h in range(2):
                order = jnp.full((size, 128), 2 * y + h + 1, jnp.int32).astype(f32)
                slope = jnp.exp2(order * (-8.0 / (2 * Y)))[:, :1]
                mask[g][h, pl.ds(start, size), :] = jnp.where(ok, jnp.exp(-slope * far), 0.0)

    def combine(zz):
        zz = lax.rem(zz + 2 * Z, Z)
        for j in range(X):
            both = jnp.concatenate(
                [wbuf[0, zz, j].astype(f32), wbuf[1, zz, j].astype(f32)], axis=0
            )
            spot = pl.multiple_of((zz * X + j) * 16, 16)
            wfull[pl.ds(spot, 16), :] = both.astype(bf16)

    for j in range(1, X):
        x_copy(X - j).wait_recv()
        r_copy(0, j).start()
        l_copy(0, j).start()
    dr_copy(0).start()
    masks(0)
    place_key = (2 * z + c) * rows - REACH[2] + lax.broadcasted_iota(
        jnp.int32, (rows + 2 * REACH[2], 128), 0
    )
    inside = (place_key >= 0) & (place_key < 2 * Z * rows)
    valid[...] = jnp.where(inside, 1.0, 0.0).astype(bf16)

    def ring(k, carry):
        for j in range(X):
            r_copy(k - 1, j).wait_recv()
            r_copy(k, j).start()
            l_copy(k - 1, j).wait_recv()

            @pl.when(k < H - 1)
            def _():
                l_copy(k, j).start()

        dr_copy(k).start()
        dl_copy(k).start()
        masks(k)
        dr_copy(k - 1).wait_recv()
        combine(z - k + 1)

        @pl.when(k > 1)
        def _():
            dl_copy(k - 1).wait_recv()
            combine(z + k - 1)

        return carry

    lax.fori_loop(1, H, ring, 0)
    for j in range(X):
        r_copy(H - 1, j).wait_recv()
    dr_copy(H).start()
    dr_copy(H - 1).wait_recv()
    combine(z - H + 1)
    dl_copy(H - 1).wait_recv()
    combine(z + H - 1)

    for k in range(X):
        @pl.when((mine == c) & (place == k))
        def _():
            own_copy.wait()

        @pl.when((mine != c) | (place != k))
        def _():
            remote(inputs.at[0], xbuf.at[k], in_send.at[0], in_recv.at[k], at(0, 1)).wait_recv()

        value = xbuf[k].astype(f32)
        mean = jnp.mean(value * value, axis=-1, keepdims=True)
        xn[pl.ds(k * L, L), :] = (value * lax.rsqrt(mean + eps) * norm_gain[...]).astype(bf16)

    dr_copy(H).wait_recv()
    combine(z - H)

    def y_copy(j):
        t = lax.rem(y + j, Y)
        spot = pl.multiple_of(t * cols, cols)
        return remote(
            wfull.at[pl.ds(spot, cols), pl.ds(wide, 128)], wo.at[y],
            y_send.at[j], y_recv.at[j], at(0, 0, 0, j),
        )

    for j in range(1, Y):
        y_copy(j).start()
    wo[y] = wfull[pl.ds(pl.multiple_of(y * cols, cols), cols), wide:]

    chain = 2 * z + c
    has_left = chain > 0
    has_right = chain < 2 * Z - 1
    left = {"z": lax.rem(z + c - 1 + Z, Z), "x": x, "c": 1 - c, "y": y}
    right = {"z": lax.rem(z + c, Z), "x": x, "c": 1 - c, "y": y}
    same = (
        (lax.broadcasted_iota(jnp.int32, (128, 128), 0) < 64)
        == (lax.broadcasted_iota(jnp.int32, (128, 128), 1) < 64)
    )
    pick = jnp.where(same, 1.0, 0.0).astype(bf16)

    def to_right(g):
        reach = REACH[g]
        return remote(
            kv[g].at[:, pl.ds(rows, reach), :], kv[g].at[:, pl.ds(0, reach), :],
            h_send.at[g, 0], h_recv.at[g, 0], right,
        )

    def to_left(g):
        reach = REACH[g]
        return remote(
            kv[g].at[:, pl.ds(reach, reach), :], kv[g].at[:, pl.ds(reach + rows, reach), :],
            h_send.at[g, 1], h_recv.at[g, 1], left,
        )

    for g in (2, 1, 0):
        reach = REACH[g]

        def project(i, carry, g=g, reach=reach):
            start = pl.multiple_of(i * 256, 256)
            block = jnp.dot(
                xn[pl.ds(start, 256), :], wfull[:, g * 384 : (g + 1) * 384],
                preferred_element_type=f32,
            ).astype(bf16).astype(f32)
            for t in range(3):
                part = block[:, t * 128 : (t + 1) * 128]
                square = part * part
                high = square.astype(bf16)
                rest = (square - high.astype(f32)).astype(bf16)
                total = jnp.dot(high, pick, preferred_element_type=f32) + jnp.dot(
                    rest, pick, preferred_element_type=f32
                )
                scaled = part * (
                    lax.rsqrt(total * (1.0 / 64) + eps) * gains[pl.ds(g * 3 + t, 1), :]
                )
                if t == 0:
                    qbuf[g, pl.ds(start, 256), :] = scaled.astype(bf16)
                else:
                    chosen = jnp.where(low if t == 2 else ~low, scaled, part)
                    kv[g][t - 1, pl.ds(start + reach, 256), :] = chosen.astype(bf16)
            return carry

        lax.fori_loop(0, rows // 256, project, 0)

        @pl.when(has_right)
        def _():
            to_right(g).start()

        @pl.when(has_left)
        def _():
            to_left(g).start()

        @pl.when(jnp.logical_not(has_left))
        def _():
            kv[g][:, pl.ds(0, reach), :] = jnp.zeros((2, reach, 128), bf16)

        @pl.when(jnp.logical_not(has_right))
        def _():
            kv[g][:, pl.ds(reach + rows, reach), :] = jnp.zeros((2, reach, 128), bf16)

    for g in (2, 1, 0):
        @pl.when(has_left)
        def _():
            to_right(g).wait_recv()

        @pl.when(has_right)
        def _():
            to_left(g).wait_recv()

    def o_copy(k, j):
        target = {
            "z": z, "x": c * half_x + k // 2, "c": lax.rem(k, 2), "y": lax.rem(y + j, Y)
        }
        return remote(
            mout.at[k], mbuf.at[y, x], o_send.at[k, j], o_recv.at[y, x], target
        )

    def is_own(k):
        return (c * half_x + k // 2 == x) & (lax.rem(k, 2) == c)

    def attend(k, carry):
        base = pl.multiple_of(k * L, L)
        sums = []
        for h in range(2):
            total = jnp.zeros((L, 256), f32)
            for g in range(3):
                reach = REACH[g]
                span = L + 2 * reach
                query = qbuf[g, pl.ds(base, L), :]
                query = jnp.where(low if h == 1 else ~low, query, jnp.zeros_like(query))
                pair = kv[g][h, pl.ds(base, span), :]
                score = lax.dot_general(
                    query, pair, (((1,), (1,)), ((), ())), preferred_element_type=f32
                )
                weight = (jnp.exp2(score) * mask[g][h]).astype(bf16)
                ones = valid[pl.ds(base + REACH[2] - reach, span), :]
                total += jnp.dot(
                    weight, jnp.concatenate([pair, ones], axis=1), preferred_element_type=f32
                )
            sums.append(total[:, :128] / total[:, 128:])
        merged = jnp.where(low, sums[0], sums[1]).astype(bf16)
        mout[k] = merged

        @pl.when(is_own(k))
        def _():
            mbuf[y, x] = merged

        @pl.when(jnp.logical_not(is_own(k)))
        def _():
            o_copy(k, 0).start()

        for j in range(1, Y):
            o_copy(k, j).start()
        return carry

    lax.fori_loop(0, X, attend, 0)

    for j in range(1, Y):
        y_copy(Y - j).wait_recv()

    total = None
    for j in range(Y):
        t = lax.rem(y + j, Y)
        for b in range(X):
            def arrive():
                remote(mout.at[0], mbuf.at[t, b], o_send.at[0, 0], o_recv.at[t, b], at(0, 1)).wait_recv()

            if j == 0:
                pl.when((b != x) | (mine != c))(arrive)
            else:
                arrive()
        part = lax.dot_general(
            mbuf[t].reshape(X * L, 128), wo[t], (((1,), (1,)), ((), ())),
            preferred_element_type=f32,
        )
        total = part if total is None else total + part
    out[...] = total.reshape(X, L, cols).astype(bf16)

    for j in range(1, X):
        x_copy(j).wait_send()
        in_copy(j).wait_send()

    @pl.when(mine != c)
    def _():
        in_copy(0).wait_send()

    def sent(k, carry):
        for j in range(X):
            r_copy(k, j).wait_send()

            @pl.when(k < H - 1)
            def _():
                l_copy(k, j).wait_send()

        dr_copy(k).wait_send()

        @pl.when(k > 0)
        def _():
            dl_copy(k).wait_send()

        return carry

    lax.fori_loop(0, H, sent, 0)
    dr_copy(H).wait_send()
    for j in range(1, Y):
        y_copy(j).wait_send()
    for g in range(3):
        @pl.when(has_right)
        def _():
            to_right(g).wait_send()

        @pl.when(has_left)
        def _():
            to_left(g).wait_send()

    def left_out(k, carry):
        for j in range(1, Y):
            o_copy(k, j).wait_send()

        @pl.when(jnp.logical_not(is_own(k)))
        def _():
            o_copy(k, 0).wait_send()

        return carry

    lax.fori_loop(0, X, left_out, 0)


def layer(inputs, norm_gain, query_weight, key_weight, value_weight, query_gain, key_gain, out_weight):
    batch, L, D = inputs.shape
    Z, X, Y = (lax.axis_size(a) for a in ("z", "x", "y"))
    depth = query_weight.shape[0]
    parts = []
    for g in range(3):
        q, k, v = query_weight[:, g], key_weight[:, g], value_weight[:, g]
        parts += [q[:, 1], q[:, 0], v[:, 0], k[:, 0], k[:, 1], v[:, 1]]
    parts.append(out_weight.reshape(128, depth).T)
    weights = jnp.concatenate(parts, axis=1)
    scale = math.log2(math.e) / 8.0
    one = jnp.ones((64,), f32)
    tiles = []
    for g in range(3):
        tiles += [
            jnp.concatenate([query_gain[g], query_gain[g]]) * scale,
            jnp.concatenate([one, key_gain[g]]),
            jnp.concatenate([key_gain[g], one]),
        ]
    gains = jnp.stack(tiles)
    rows = X * L
    H = Z // 2
    dma = pltpu.SemaphoreType.DMA
    vmem = pl.BlockSpec(memory_space=pltpu.VMEM)
    cols = D // Y
    return pl.pallas_call(
        functools.partial(kernel, Z, X, Y, L),
        out_shape=jax.ShapeDtypeStruct((batch, L, cols), bf16),
        in_specs=[pl.BlockSpec(memory_space=pl.ANY), vmem, vmem, vmem],
        out_specs=vmem,
        scratch_shapes=[
            pltpu.VMEM((X, L, D), bf16),
            pltpu.VMEM((2, Z, X, 8, 1280), bf16),
            pltpu.VMEM((D, 1280), bf16),
            pltpu.VMEM((rows, D), bf16),
            pltpu.VMEM((3, rows, 128), bf16),
            *(pltpu.VMEM((2, rows + 2 * r, 128), bf16) for r in REACH),
            pltpu.VMEM((rows + 2 * REACH[2], 128), bf16),
            *(pltpu.VMEM((2, L, L + 2 * r), f32) for r in REACH),
            pltpu.VMEM((X, L, 128), bf16),
            pltpu.VMEM((Y, X, L, 128), bf16),
            pltpu.VMEM((Y, cols, 128), bf16),
            dma((X,)), dma((X,)), dma((X,)), dma((X,)), dma,
            dma((H, X)), dma((H, X)), dma((H, X)), dma((H, X)),
            dma((H + 1,)), dma((H + 1,)), dma((H + 1,)), dma((H + 1,)),
            dma((3, 2)), dma((3, 2)), dma((X, Y)), dma((Y, X)), dma((Y,)), dma((Y,)),
        ],
        compiler_params=pltpu.CompilerParams(
            collective_id=0, has_side_effects=True, vmem_limit_bytes=60 * 1024 * 1024
        ),
        name="layer",
    )(inputs, weights, norm_gain.reshape(1, D), gains)


def solution(mesh):
    count = mesh.shape["sp"]
    X = 4
    finer = Mesh(
        mesh.devices.reshape(count // (2 * X), X, 2, mesh.shape["tp"]), ("z", "x", "c", "y")
    )
    placed = (
        P(None, SP, None),
        P(),
        P(SP, None, "y", None),
        P(SP, None, "y", None),
        P(SP, None, "y", None),
        P(),
        P(),
        P("y", None, SP),
    )
    return jax.shard_map(
        layer, mesh=finer, in_specs=placed, out_specs=P(None, SP, "y"), check_vma=False
    )
```

time: 475 us -> 76.7 us (0.16)
  the two profiles are of different devices: /device:TPU:1 before, /device:TPU:3 now
where the time goes in v1:
time: 76.7 us; the launch traced here: 76.3 us
  Pallas kernels  69.3 us (90%)
  local copies, waits for them, and re-layouts  6.73 us (9%)
    pallas_call x1, Pallas kernels, layer(): pl.pallas_call(functools.partial(kernel, Z, X, Y, L), out_shape=jax.Shape...  69.3 us
    unnamed x15, local copies, waits for them, and re-layouts  3.74 us

profile of v1, /device:TPU:3, one launch (start us, length us, event | category | flops | bytes accessed | tf_op | source)
XLA Modules:
  0.0 76.3 jit_solution(17217763405357758432)
XLA Ops:
  0.0 0.8 %fusion.3 = (f32[1,64]{1,0:T(1,128)S(1)}, f32[1,64]{1,0:T(1,128)S(1)}, f32[1,64]{1,0:T(1,128)S(1)}) fusion(f32[3,64]{1,0:T(4,128)} %param.13), kind=kLoop, calls=%fused_computation.42 | loop fusion | bytes 1536 | tf_op jit(solution)/shard_map/slice | solution.py:435
  0.8 0.1 maximum_multiply_fusion.2
  0.9 0.1 maximum_multiply_fusion
  0.9 0.0 copy-start.4
  1.0 0.7 copy-done.4
  1.6 0.1 pad_bitcast_fusion
  1.7 0.1 pad_bitcast_fusion.4
  1.8 0.0 copy-start.3
  1.8 0.0 copy-start
  1.8 1.2 %stack.30.gains = f32[9,128]{1,0:T(8,128)} concatenate(f32[1,128]{1,0:T(1,128)S(1)} %get-tuple-element.52, f32[1,128]{1,0:T(1,128)S(1)} %get-tuple-element.43, f32[1,128]{1,0:T(1,128)S(1)} %get-tuple-element.42, f32[1,128]{1,0:T(1,128)S(1)} %get-tuple-element.53, f32[1,128]{1,0:T(1,128)S(1)} %get-tuple-element.54, f32[1,128]{1,0:T(1,128)S(1)} %get-tuple-element.55, ...), dimensions={0} | concatenate | bytes 9216 | tf_op jit(solution)/shard_map/stack | solution.py:439
  3.0 0.0 copy-done.3
  3.0 0.1 reshape.81
  3.1 0.0 copy-done
  3.1 0.0 copy-start.1
  3.2 0.7 copy-done.1
  3.9 0.0 copy-start.2
  3.9 0.7 copy-done.2
  4.7 0.7 concatenate.51.weights
  5.4 69.3 %layer.1 = bf16[4,128,256]{2,1,0:T(8,128)(2,1)} custom-call(bf16[4,128,1024]{2,1,0:T(8,128)(2,1)} %inputs.1, bf16[8,1280]{1,0:T(8,128)(2,1)} %concatenate.51.weights, f32[1,1024]{1,0:T(1,128)} %bitcast.83, f32[9,128]{1,0:T(8,128)} %stack.30.gains), custom_call_target="tpu_custom_call" | custom-call | tf_op jit(solution)/shard_map/layer/pallas_call | solution.py:445
  74.7 1.7 %copy.41 = bf16[4,128,256]{2,1,0:T(8,128)(2,1)} copy(bf16[4,128,256]{2,1,0:T(8,128)(2,1)} %layer.1) | data formatting | bytes 524288
  (19 shorter events, 0.1 us)
Async XLA Ops:
  0.9 0.7 copy-start.4
  1.8 1.2 %copy-start.3 = (bf16[2,64,8]{1,2,0:T(8,128)(2,1)S(1)}, bf16[2,64,8]{1,2,0:T(8,128)(2,1)}, u32[]{:S(2)}) copy-start(bf16[2,64,8]{1,2,0:T(8,128)(2,1)} %param.15) | copy-start | bytes 6148
  1.8 1.3 %copy-start = (bf16[8,3,2,64]{3,2,1,0:T(2,128)(2,1)S(1)}, bf16[8,3,2,64]{3,2,1,0:T(2,128)(2,1)}, u32[]{:S(2)}) copy-start(bf16[8,3,2,64]{3,2,1,0:T(2,128)(2,1)} %param.10) | copy-start | bytes 18436
  3.1 0.7 copy-start.1
  3.9 0.7 copy-start.2
